TPU v7x, 32 devices: a whole 2x2x4 slice. The times are simulated.
32 devices in a mesh: ep: 8 (over z, x), tp: 4 (over y, core).
Axes of the slice: x: 2, y: 2, z: 4, core: 2. Of those that a mesh axis runs over, the one named last changes fastest.
Arguments:
- mix_query: bfloat16 [16384, 2048], P('ep', 'tp'), may hold values from -6 to 6
- mix_key: bfloat16 [16384, 2048], P('ep', 'tp'), may hold values from -6 to 6
- mix_value: bfloat16 [16384, 2048], P('ep', 'tp'), may hold values from -6 to 6
- mix_gate: bfloat16 [16384, 2048], P('ep', 'tp'), may hold values from -6 to 6
- log_decay: float32 [16384, 8], P('ep', 'tp'), may hold values from -1 to 0, as said below
- ret_gain: float32 [2048], P('tp'), may hold values from 0.1 to 1.9
- w_out: bfloat16 [2048, 2048], replicated, may hold values from -0.125 to 0.125
- moe_in: bfloat16 [1024, 2048], P(('ep', 'tp')), may hold values from -6 to 6
- route_ids: int32 [1024, 2], P(('ep', 'tp')), may hold values from 0 to 7, as said below
- route_weights: float32 [1024, 2], P(('ep', 'tp')), may hold values from 0.1 to 1
- moe_gain: float32 [2048], replicated, may hold values from 0.1 to 1.9
- w_gate: bfloat16 [8, 2048, 7168], P('ep', None, 'tp'), may hold values from -0.125 to 0.125
- w_up: bfloat16 [8, 2048, 7168], P('ep', None, 'tp'), may hold values from -0.125 to 0.125
- w_down: bfloat16 [8, 7168, 2048], P('ep', 'tp'), may hold values from -0.0625 to 0.0625
Outputs:
- mix_out: bfloat16 [16384, 2048], P(('ep', 'tp'))
- moe_out: bfloat16 [1024, 2048], P(('ep', 'tp'))
Inputs may be any that keep to these rules, and one draw needn't show every extreme that they name: `log_decay`: log of a decay. `route_ids`: each row names 2 different experts. Among the rows of one device no expert is named by more than 16 rows, and one expert is named by exactly 16 rows of every device.
All inputs are finite; a program needn't handle non-finite values.
Results may differ from a plain program's by a relative error of at most 0.015.
Values may be sent and summed in bfloat16 or wider, within the bound.
A program may use at most 128 MiB of HBM per device.

v0:
```python
import jax
import jax.numpy as jnp
from jax import lax
from jax.sharding import PartitionSpec as P

HEAD_DIM = 256
BLOCK = 512
norm_eps = 1e-06


def prefix(x, axis, join, neutral):
    place = lax.axis_index(axis)
    gathered = jax.tree.map(
        lambda a, kind: lax.all_gather(a.astype(kind), axis), x, (jnp.bfloat16, jnp.bfloat16)
    )
    state = jax.tree.map(lambda a, e: jnp.zeros_like(a) + jnp.asarray(e, a.dtype), x, neutral)

    def one(hop, state):
        return join(
            state,
            jax.tree.map(
                lambda a, own: lax.dynamic_index_in_dim(a, hop, 0, False).astype(own.dtype),
                gathered,
                x,
            ),
        )

    return lax.fori_loop(0, place, one, state)


def rotate(tensor, position_index):
    head_dim = tensor.shape[-1]
    half_dim = head_dim // 2
    inverse = 10000.0 ** (-(jnp.arange(half_dim, dtype=jnp.float32) * 2.0) / head_dim)
    angle = position_index.astype(jnp.float32)[:, None] * inverse[None, :]
    cosine = jnp.cos(angle)[:, None, :]
    sine = jnp.sin(angle)[:, None, :]
    front = tensor[..., :half_dim]
    back = tensor[..., half_dim:]
    return jnp.concatenate([front * cosine - back * sine, back * cosine + front * sine], axis=-1)


def chain(earlier, later):
    return (earlier[0] * later[0], later[0][:, None, None] * earlier[1] + later[1])


def carry_block(carried, block_items):
    update, block_last = block_items
    return (jnp.exp(block_last)[:, None, None] * carried + update, carried)


def mixer_half(mix_query, mix_key, mix_value, mix_gate, log_decay, ret_gain, w_out):
    seq_rows = mix_query.shape[0]
    local_heads = mix_query.shape[1] // HEAD_DIM
    block_count = seq_rows // BLOCK
    position_index = lax.axis_index("ep") * seq_rows + jnp.arange(seq_rows, dtype=jnp.int32)
    query_rot = rotate(
        mix_query.astype(jnp.float32).reshape(seq_rows, local_heads, HEAD_DIM), position_index
    ).astype(jnp.bfloat16)
    key_rot = (
        rotate(mix_key.astype(jnp.float32).reshape(seq_rows, local_heads, HEAD_DIM), position_index)
        * HEAD_DIM ** (-0.5)
    ).astype(jnp.bfloat16)
    query_blocks = query_rot.reshape(block_count, BLOCK, local_heads, HEAD_DIM)
    key_blocks = key_rot.reshape(block_count, BLOCK, local_heads, HEAD_DIM)
    value_blocks = mix_value.reshape(block_count, BLOCK, local_heads, HEAD_DIM)
    cumulative = jnp.cumsum(log_decay.reshape(block_count, BLOCK, local_heads), axis=1)
    causal = jnp.arange(BLOCK)[:, None] >= jnp.arange(BLOCK)[None, :]
    scores = jnp.einsum(
        "nihd,njhd->nhij", query_blocks, key_blocks, preferred_element_type=jnp.float32
    )
    by_head = jnp.transpose(cumulative, (0, 2, 1))
    log_gap = by_head[:, :, :, None] - by_head[:, :, None, :]
    decay_mask = jnp.where(causal, jnp.exp(jnp.where(causal, log_gap, 0.0)), 0.0)
    weights = (scores * decay_mask).astype(jnp.bfloat16)
    within_block = jnp.einsum(
        "nhij,njhe->nihe", weights, value_blocks, preferred_element_type=jnp.float32
    )
    block_last = cumulative[:, -1, :]
    key_decayed = (
        key_blocks.astype(jnp.float32) * jnp.exp(block_last[:, None, :] - cumulative)[..., None]
    ).astype(jnp.bfloat16)
    updates = jnp.einsum(
        "njhd,njhe->nhde", key_decayed, value_blocks, preferred_element_type=jnp.float32
    )
    empty_state = jnp.zeros((local_heads, HEAD_DIM, HEAD_DIM), jnp.float32)
    local_end, starts = lax.scan(carry_block, empty_state, (updates, block_last))
    through = jnp.cumsum(block_last, axis=0)
    before = through - block_last
    incoming = prefix(
        (jnp.exp(through[-1]), local_end), "ep", chain, (jnp.ones_like(through[-1]), empty_state)
    )
    block_states = starts + jnp.exp(before)[:, :, None, None] * incoming[1][None]
    query_decayed = query_blocks.astype(jnp.float32) * jnp.exp(cumulative)[..., None]
    carried_part = jnp.einsum(
        "nihd,nhde->nihe", query_decayed, block_states, precision=lax.Precision.HIGHEST
    )
    retained = (within_block + carried_part).reshape(seq_rows, local_heads, HEAD_DIM)
    inverse_rms = lax.rsqrt(jnp.mean(retained * retained, axis=-1, keepdims=True) + norm_eps)
    gate_act = jax.nn.silu(mix_gate.astype(jnp.float32).reshape(seq_rows, local_heads, HEAD_DIM))
    heads_out = (
        gate_act * retained * inverse_rms * ret_gain.reshape(local_heads, HEAD_DIM)
    ).astype(jnp.bfloat16)
    by_rows = lax.all_to_all(
        heads_out.reshape(seq_rows, local_heads * HEAD_DIM),
        "tp",
        split_axis=0,
        concat_axis=1,
        tiled=True,
    )
    return jnp.dot(by_rows, w_out, preferred_element_type=jnp.float32).astype(jnp.bfloat16)


def expert_half(moe_in, route_ids, route_weights, moe_gain, w_gate, w_up, w_down):
    tokens, model_width = moe_in.shape
    route_count = route_ids.shape[1]
    experts = lax.axis_size("ep")
    lane_count = lax.axis_size("tp")
    capacity = 4 * tokens // experts
    floats = moe_in.astype(jnp.float32)
    normed = (
        floats * lax.rsqrt(jnp.mean(floats * floats, axis=-1, keepdims=True) + norm_eps) * moe_gain
    ).astype(jnp.bfloat16)
    flat_ids = route_ids.reshape(-1)
    onehot = (flat_ids[:, None] == jnp.arange(experts, dtype=jnp.int32)[None, :]).astype(jnp.int32)
    slot_index = jnp.sum(jnp.cumsum(onehot, axis=0) * onehot, axis=1) - 1
    target = flat_ids * capacity + slot_index
    source = jnp.arange(tokens * route_count, dtype=jnp.int32) // route_count
    slot_owner = jnp.full((experts * capacity,), tokens, jnp.int32).at[target].set(source)
    padded = jnp.concatenate([normed, jnp.zeros((1, model_width), jnp.bfloat16)], axis=0)
    outgoing = padded[slot_owner]
    gate_weight = w_gate[0]
    up_weight = w_up[0]
    down_weight = w_down[0]
    copies = jnp.broadcast_to(
        outgoing.reshape(experts, 1, capacity, model_width),
        (experts, lane_count, capacity, model_width),
    )
    arrived = lax.all_to_all(
        copies.reshape(experts * lane_count * capacity, model_width),
        ("ep", "tp"),
        split_axis=0,
        concat_axis=0,
        tiled=True,
    )
    gate_part = jnp.dot(arrived, gate_weight, preferred_element_type=jnp.float32)
    up_part = jnp.dot(arrived, up_weight, preferred_element_type=jnp.float32)
    hidden_grid = (
        (jax.nn.silu(gate_part) * up_part)
        .astype(jnp.bfloat16)
        .reshape(experts, lane_count, capacity, -1)
    )
    partial_value = jnp.einsum(
        "elcf,fd->lecd", hidden_grid, down_weight, preferred_element_type=jnp.float32
    )
    summed_rows = lax.psum_scatter(
        partial_value.reshape(lax.axis_size("tp") * (experts * capacity), model_width).astype(
            jnp.bfloat16
        ),
        "tp",
        scatter_dimension=0,
        tiled=True,
    )
    returned = lax.all_to_all(summed_rows, "ep", split_axis=0, concat_axis=0, tiled=True)
    picked_rows = returned[target].reshape(tokens, route_count, model_width)
    combined = jnp.sum(picked_rows.astype(jnp.float32) * route_weights[:, :, None], axis=1)
    return combined.astype(jnp.bfloat16)


def on_device(
    mix_query,
    mix_key,
    mix_value,
    mix_gate,
    log_decay,
    ret_gain,
    w_out,
    moe_in,
    route_ids,
    route_weights,
    moe_gain,
    w_gate,
    w_up,
    w_down,
):
    mix_out = mixer_half(mix_query, mix_key, mix_value, mix_gate, log_decay, ret_gain, w_out)
    moe_out = expert_half(moe_in, route_ids, route_weights, moe_gain, w_gate, w_up, w_down)
    return (mix_out, moe_out)


def solution(mesh):
    in_specs = (
        P("ep", "tp"),
        P("ep", "tp"),
        P("ep", "tp"),
        P("ep", "tp"),
        P("ep", "tp"),
        P("tp"),
        P(),
        P(("ep", "tp"), None),
        P(("ep", "tp"), None),
        P(("ep", "tp"), None),
        P(),
        P("ep", None, "tp"),
        P("ep", None, "tp"),
        P("ep", "tp", None),
    )
    out_specs = (P(("ep", "tp"), None), P(("ep", "tp"), None))
    return jax.shard_map(
        on_device, mesh=mesh, in_specs=in_specs, out_specs=out_specs, check_vma=False
    )
```

profile of v0, /device:TPU:0, one launch (start us, length us, event | category | flops | bytes accessed | tf_op | source)
XLA Modules:
  0.0 214.7 jit_solution(8959980904177569203)
XLA Ops:
  8.0 0.8 copy.193
  8.8 0.7 broadcast_multiply_fusion
  9.6 0.1 reduce_window_sum.48
  9.7 0.2 select_reduce_fusion
  10.0 0.1 mul.276
  10.1 0.8 scatter_custom_fusion
  10.9 1.0 fusion.51
  12.0 1.0 fusion.53
  13.0 0.9 gather_fusion
  14.0 1.6 broadcast_in_dim.38
  15.6 7.5 %all-to-all-start.1 = ((bf16[32,16,2048]{2,1,0:T(8,128)(2,1)}), bf16[32,16,2048]{2,1,0:T(8,128)(2,1)}, u32[]{:S(2)}, u32[]{:S(2)}) async-start(bf16[32,16,2048]{2,1,0:T(8,128)(2,1)} %bitcast.23), calls=%async_computation.1 | async-start | bytes 4194304 | tf_op jit(solution)/shard_map/all_to_all | solution.py:139
  23.2 2.4 %reduce-window.6 = f32[4,2,4,128]{3,2,1,0:T(4,128)S(1)} reduce-window(f32[4,2,4,128]{3,2,1,0:T(4,128)S(1)} %copy.201, f32[]{:T(128)} %constant.91.clone.1), window={size=1x1x1x128 pad=0_0x0_0x0_0x127_0}, to_apply=%region_0.0 | reduce-window | flops 520192 | bytes 32772 | tf_op jit(solution)/shard_map/reduce-window
  25.6 0.2 slice_reduce_fusion
  25.8 0.7 reduce-window.9
  26.6 0.2 slice_reduce_fusion.1
  26.9 2.9 %copy.165 = bf16[2048,512]{0,1:T(8,128)(2,1)S(1)} copy(bf16[2048,512]{1,0:T(8,128)(2,1)} %param.18) | data formatting | bytes 4194304 | tf_op args[0]
  29.8 2.5 %convert.15 = f32[2048,2,256]{0,2,1:T(8,128)} convert(bf16[2048,2,256]{0,2,1:T(8,128)(2,1)S(1)} %bitcast.104) | non-fusion elementwise | flops 1048576 | bytes 6291456 | tf_op jit(solution)/shard_map/reshape | solution.py:58
  32.3 2.9 %copy.170 = bf16[2048,512]{0,1:T(8,128)(2,1)S(1)} copy(bf16[2048,512]{1,0:T(8,128)(2,1)} %param.19) | data formatting | bytes 4194304 | tf_op args[1]
  35.2 0.5 convert.16
  35.7 3.7 %multiply_cosine_fusion = (f32[2048,128]{0,1:T(8,128)S(1)}, f32[2048,128]{0,1:T(8,128)S(1)}) fusion(f32[128]{0:T(128)S(1)} %multiply_power_fusion, f32[2048]{0:T(1024)S(1)} %add_convert_fusion.1), kind=kLoop, calls=%fused_computation.61 | loop fusion | flops 262144 | bytes 2105856 | tf_op jit(solution)/shard_map/cos | solution.py:36
  39.5 3.1 %multiply_subtract_fusion = (f32[2048,2,128]{0,2,1:T(8,128)}, f32[2048,2,128]{0,2,1:T(8,128)S(1)}, bf16[2048,2,128]{0,2,1:T(8,128)(2,1)S(1)}, bf16[2048,2,128]{0,2,1:T(8,128)(2,1)}) fusion(f32[2048,2,256]{0,2,1:T(8,128)S(1)} %convert.16, f32[2048,128]{0,1:T(8,128)S(1)} %get-tuple-element.194, f32[2048,128]{0,1:T(8,128)S(1)} %get-tuple-element.193, ...), kind=kLoop, calls=%fused_computation.53 | loop fusion | flops 7340032 | bytes 16777216 | tf_op jit(solution)/shard_map/sub | solution.py:40
  42.5 2.9 %copy.171 = f32[2048,2,128]{2,0,1:T(8,128)} copy(f32[2048,2,128]{0,2,1:T(8,128)} %get-tuple-element.185) | data formatting | bytes 4194304 | tf_op jit(solution)/shard_map/sub | solution.py:40
  45.4 1.8 copy.172
  47.3 4.2 %reshape.244 = bf16[4,512,2,256]{3,2,1,0:T(2,128)(2,1)} reshape(bf16[2048,512]{1,0:T(8,128)(2,1)} %param.20) | data formatting | bytes 4194304 | tf_op jit(solution)/shard_map/reshape | solution.py:66
  51.4 5.1 %fusion.36 = f32[4,2,256,256]{3,2,1,0:T(8,128)} fusion(f32[4,512,2]{1,2,0:T(2,128)S(1)} %copy.180, bf16[4,512,2,256]{3,2,1,0:T(2,128)(2,1)} %reshape.244, f32[4,512,2,128]{3,1,0,2:T(8,128)} %bitcast.115, f32[4,512,2,128]{3,1,0,2:T(8,128)S(1)} %bitcast.114), kind=kOutput, calls=%fused_computation.46 | convolution fusion | flops 543162368 | bytes 8404992 | tf_op jit(solution)/shard_map/njhd,njhe->nhde/dot_general | solution.py:83
  56.6 8.1 %while.26 = (s32[]{:T(128)}, f32[2,256,256]{2,1,0:T(8,128)S(1)}, f32[4,2,256,256]{3,2,1,0:T(8,128)}, f32[4,2]{1,0:T(4,128)S(1)}, f32[4,2,256,256]{3,2,1,0:T(8,128)}, /*index=5*/s32[]{:T(128)}, s32[]{:T(128)}) while((s32[]{:T(128)}, f32[2,256,256]{2,1,0:T(8,128)S(1)}, f32[4,2,256,256]{3,2,1,0:T(8,128)}, f32[4,2]{1,0:T(4,128)S(1)}, ...), condition=%wide.region_3.4_spmd.clone, body=%wide.region_2.3_spmd.clone.sunk | while | flops 524291 | bytes 2622072 | solution.py:87
  56.6 0.8 bitcast_dynamic-update-slice_fusion.2
  57.5 1.2 bitcast_add_fusion.4
  58.6 0.8 bitcast_dynamic-update-slice_fusion.2
  59.5 1.2 bitcast_add_fusion.4
  60.7 0.8 bitcast_dynamic-update-slice_fusion.2
  61.5 1.2 bitcast_add_fusion.4
  62.7 0.8 bitcast_dynamic-update-slice_fusion.2
  63.5 1.2 bitcast_add_fusion.4
  64.7 0.7 convert_element_type.100
  65.5 0.2 reduce_window_sum.47
  65.7 0.2 fusion.55
  65.9 20.9 %all-gather.1 = bf16[8,1,2]{2,1,0:T(2,128)(2,1)S(1)} all-gather(bf16[1,1,2]{2,1,0:T(2,128)(2,1)S(1)} %bitcast.125), channel_id=1, replica_groups=mesh['ep'=8,'tp'=4] {'ep'}, dimensions={0}, use_global_device_ids=true | all-gather | bytes 36 | tf_op jit(solution)/shard_map/all_gather | solution.py:14
  86.9 0.7 copy.166
  87.5 0.7 copy.167
  88.4 7.5 %fusion.14 = f32[4,2,512,256]{2,3,1,0:T(8,128)} fusion(f32[4,2,512]{2,1,0:T(2,128)S(1)} %reshape.284, pred[512,512]{1,0:T(8,128)(4,1)S(1)} %iota_compare_fusion, bf16[4,512,2,256]{3,2,1,0:T(2,128)(2,1)} %reshape.244, f32[4,512,2,128]{3,1,0,2:T(8,128)} %bitcast.116, f32[4,512,2,128]{3,1,0,2:T(8,128)} %bitcast.113, ...), kind=kOutput, calls=%fused_computation.26 | convolution fusion | flops 2165309440 | bytes 12861440 | tf_op jit(solution)/shard_map/nhij,njhe->nihe/dot_general | solution.py:76
  95.9 7.8 %fusion.6 = f32[512,1792]{1,0:T(8,128)S(1)} fusion(bf16[512,2048]{1,0:T(8,128)(2,1)} %bitcast.24, bf16[1,2048,1792]{2,1,0:T(8,128)(2,1)} %param.29), kind=kOutput, calls=%fused_computation.16 | convolution fusion | flops 3758096384 | bytes 13107200 | tf_op jit(solution)/shard_map/dot_general | solution.py:146
  103.8 8.0 %multiply_convert_fusion.3 = bf16[512,1792]{1,0:T(8,128)(2,1)S(1)} fusion(f32[512,1792]{1,0:T(8,128)S(1)} %fusion.6, bf16[512,2048]{1,0:T(8,128)(2,1)} %bitcast.24, bf16[1,2048,1792]{2,1,0:T(8,128)(2,1)} %param.30), kind=kOutput, calls=%fused_computation.41 | convolution fusion | flops 3763601408 | bytes 14942208 | tf_op jit(solution)/shard_map/dot_general | solution.py:147
  111.9 4.2 %fusion.31 = bf16[4,8,16,2048]{3,2,0,1:T(8,128)(2,1)S(1)} fusion(bf16[8,4,16,1792]{3,2,1,0:T(8,128)(2,1)S(1)} %bitcast.128, bf16[1,1792,2048]{2,1,0:T(8,128)(2,1)S(1)} %bitcast.127), kind=kOutput, calls=%fused_computation.45 | convolution fusion | flops 3759144960 | bytes 11272192 | tf_op jit(solution)/shard_map/elcf,fd->lecd/dot_general | solution.py:153
  116.0 1.6 copy.194
  117.7 0.2 while.25
  118.0 11.4 %multiply_reduce_fusion = (f32[4,512,2]{1,2,0:T(2,128)S(1)}, f32[4,512,2,256]{1,3,2,0:T(8,128)}) fusion(f32[4,512,2]{1,2,0:T(2,128)S(1)} %copy.187, f32[4,2,256,256]{3,2,1,0:T(8,128)} %get-tuple-element.74, f32[2,256,256]{2,1,0:T(8,128)S(1)} %get-tuple-element.76, f32[4,2]{1,0:T(4,128)S(1)} %copy.184, f32[4,2,512,256]{2,3,1,0:T(8,128)} %fusion.14, ...), kind=kOutput, calls=%fused_computation.31 | convolution fusion | flops 3231707136 | bytes 13140000 | tf_op jit(solution)/shard_map/nihd,nhde->nihe/dot_general | solution.py:95
  129.4 0.4 copy.190
  129.8 2.5 %mul.264 = f32[2048,2,256]{2,1,0:T(2,128)S(1)} broadcast(f32[2048,2]{1,0:T(8,128)S(1)} %copy.190), dimensions={0,1} | broadcast | bytes 4210688 | tf_op jit(solution)/shard_map/mul | solution.py:102
  132.3 2.4 %copy.205 = f32[256,8,2,256]{3,1,2,0:T(8,128)} copy(f32[256,8,2,256]{3,2,1,0:T(2,128)S(1)} %bitcast.99) | data formatting | bytes 8388608
  134.7 7.3 %copy.189 = f32[4,512,2,256]{3,2,1,0:T(2,128)} copy(f32[4,512,2,256]{1,3,2,0:T(8,128)} %get-tuple-element.196) | data formatting | bytes 8388608 | tf_op jit(solution)/shard_map/add | solution.py:98
  142.0 2.8 %copy.204 = f32[256,8,2,256]{3,1,2,0:T(8,128)S(1)} copy(f32[256,8,2,256]{3,2,1,0:T(2,128)} %bitcast.102) | data formatting | bytes 8388608
  144.8 0.7 copy-done
  145.5 0.7 copy-done.4
  146.1 1.6 fusion.22
  147.8 2.4 %copy.191 = bf16[4,512,512]{1,2,0:T(8,128)(2,1)} copy(bf16[4,512,512]{2,1,0:T(8,128)(2,1)S(1)} %bitcast.107) | data formatting | bytes 4194304 | tf_op jit(solution)/shard_map/all_to_all | solution.py:104
  150.2 3.7 %all-to-all-start = ((bf16[4,512,512]{1,2,0:T(8,128)(2,1)}), bf16[4,512,512]{1,2,0:T(8,128)(2,1)S(1)}, u32[]{:S(2)}, u32[]{:S(2)}) async-start(bf16[4,512,512]{1,2,0:T(8,128)(2,1)} %copy.191), calls=%async_computation | async-start | bytes 4194304 | tf_op jit(solution)/shard_map/all_to_all | solution.py:104
  154.0 25.5 %all-to-all-done = bf16[4,512,512]{1,2,0:T(8,128)(2,1)S(1)} async-done(((bf16[4,512,512]{1,2,0:T(8,128)(2,1)}), bf16[4,512,512]{1,2,0:T(8,128)(2,1)S(1)}, u32[]{:S(2)}, u32[]{:S(2)}) %all-to-all-start) | async-done | bytes 2097184 | tf_op jit(solution)/shard_map/all_to_all | solution.py:104
  179.5 11.0 %all-to-all-start.2 = ((bf16[8,16,2048]{2,1,0:T(8,128)(2,1)}), bf16[8,16,2048]{2,1,0:T(8,128)(2,1)S(1)}, u32[]{:S(2)}, u32[]{:S(2)}) async-start(bf16[8,16,2048]{2,1,0:T(8,128)(2,1)} %bitcast.119), calls=%async_computation.3 | async-start | bytes 1048576 | tf_op jit(solution)/shard_map/all_to_all | solution.py:164
  190.5 9.1 %convolution_convert_fusion = bf16[512,2048]{1,0:T(8,128)(2,1)} fusion(bf16[512,2048]{0,1:T(8,128)(2,1)S(1)} %bitcast.117, bf16[2048,2048]{1,0:T(8,128)(2,1)} %param.24), kind=kOutput, calls=%fused_computation.43 | convolution fusion | flops 4296015872 | bytes 12582912 | tf_op jit(solution)/shard_map/dot_general | solution.py:111
  199.7 5.1 %all-to-all-done.2 = bf16[8,16,2048]{2,1,0:T(8,128)(2,1)S(1)} async-done(((bf16[8,16,2048]{2,1,0:T(8,128)(2,1)}), bf16[8,16,2048]{2,1,0:T(8,128)(2,1)S(1)}, u32[]{:S(2)}, u32[]{:S(2)}) %all-to-all-start.2) | async-done | bytes 524320 | tf_op jit(solution)/shard_map/all_to_all | solution.py:164
  204.8 0.7 gather_fusion.1
  205.5 0.3 reshape.253
  205.9 1.4 multiply_reduce_fusion.1
  (61 shorter events, 1.3 us)
Async XLA Ops:
  15.6 7.5 %copy-start.5 = (f32[2048,2]{0,1:T(2,128)S(1)}, f32[2048,2]{0,1:T(2,128)}, u32[]{:S(2)}) copy-start(f32[2048,2]{0,1:T(2,128)} %param.22) | copy-start | bytes 49156
  15.6 80.4 %all-to-all-start.1 = ((bf16[32,16,2048]{2,1,0:T(8,128)(2,1)}), bf16[32,16,2048]{2,1,0:T(8,128)(2,1)}, u32[]{:S(2)}, u32[]{:S(2)}) async-start(bf16[32,16,2048]{2,1,0:T(8,128)(2,1)} %bitcast.23), calls=%async_computation.1 | async-start | bytes 4194304 | tf_op jit(solution)/shard_map/all_to_all | solution.py:139
  23.0 94.6 %all-gather.4.cloned.1.call-start = ((), (), s32[]{:S(2)}) async-start(), calls=%async_computation.5 | async-start | bytes 2359296 | tf_op jit(solution)/shard_map/all_gather | solution.py:14
  35.2 4.2 %copy-start.1 = (f32[2048,2,256]{0,2,1:T(8,128)S(1)}, f32[2048,2,256]{0,2,1:T(8,128)}, u32[]{:S(2)}) copy-start(f32[2048,2,256]{0,2,1:T(8,128)} %convert.15) | copy-start | bytes 12582916
  47.3 4.2 %copy-start.3 = (f32[2048,2,128]{2,0,1:T(8,128)S(1)}, f32[2048,2,128]{2,0,1:T(8,128)}, u32[]{:S(2)}) copy-start(f32[2048,2,128]{2,0,1:T(8,128)} %copy.171) | copy-start | bytes 6291460
  56.6 30.3 %copy-start.2 = (bf16[2048,2,128]{0,2,1:T(8,128)(2,1)S(1)}, bf16[2048,2,128]{0,2,1:T(8,128)(2,1)}, u32[]{:S(2)}) copy-start(bf16[2048,2,128]{0,2,1:T(8,128)(2,1)} %get-tuple-element.190) | copy-start | bytes 3145732
  65.4 114.1 %reduce-scatter.2.cloned.1.call-start = ((), (), s32[]{:S(2)}) async-start(), calls=%async_computation.4 | async-start | bytes 2621440 | tf_op jit(solution)/shard_map/reduce_scatter | solution.py:156
  95.9 15.9 %slice-start = ((s8[7340032]{0:T(1024)(128)(4,1)}), s8[4194304]{0:T(1024)(128)(4,1)S(1)}, s32[]{:S(2)}) async-start(s8[7340032]{0:T(1024)(128)(4,1)} %bitcast.126), calls=%async_computation.6 | async-start | bytes 8388608
  103.8 8.1 %slice-start.1 = ((s8[7340032]{0:T(1024)(128)(4,1)}), s8[3145728]{0:T(1024)(128)(4,1)S(1)}, s32[]{:S(2)}) async-start(s8[7340032]{0:T(1024)(128)(4,1)} %bitcast.126), calls=%async_computation.7 | async-start | bytes 6291456
  142.0 3.5 %copy-start = (f32[256,8,2,256]{3,1,2,0:T(8,128)S(1)}, f32[256,8,2,256]{3,1,2,0:T(8,128)}, u32[]{:S(2)}) copy-start(f32[256,8,2,256]{3,1,2,0:T(8,128)} %copy.205) | copy-start | bytes 12582916
  142.0 4.2 %copy-start.4 = (bf16[2048,512]{1,0:T(8,128)(2,1)S(1)}, bf16[2048,512]{1,0:T(8,128)(2,1)}, u32[]{:S(2)}) copy-start(bf16[2048,512]{1,0:T(8,128)(2,1)} %param.21) | copy-start | bytes 6291460
  142.0 4.2 %copy-start.6 = (f32[512]{0:T(512)S(1)}, f32[512]{0:T(512)}, u32[]{:S(2)}) copy-start(f32[512]{0:T(512)} %param.23) | copy-start | bytes 6148
  150.2 3.8 %copy-start.7 = (f32[32,2]{0,1:T(2,128)S(1)}, f32[32,2]{0,1:T(2,128)}, u32[]{:S(2)}) copy-start(f32[32,2]{0,1:T(2,128)} %param.27) | copy-start | bytes 772
  150.2 29.4 %all-to-all-start = ((bf16[4,512,512]{1,2,0:T(8,128)(2,1)}), bf16[4,512,512]{1,2,0:T(8,128)(2,1)S(1)}, u32[]{:S(2)}, u32[]{:S(2)}) async-start(bf16[4,512,512]{1,2,0:T(8,128)(2,1)} %copy.191), calls=%async_computation | async-start | bytes 4194304 | tf_op jit(solution)/shard_map/all_to_all | solution.py:104
  179.5 25.2 %all-to-all-start.2 = ((bf16[8,16,2048]{2,1,0:T(8,128)(2,1)}), bf16[8,16,2048]{2,1,0:T(8,128)(2,1)S(1)}, u32[]{:S(2)}, u32[]{:S(2)}) async-start(bf16[8,16,2048]{2,1,0:T(8,128)(2,1)} %bitcast.119), calls=%async_computation.3 | async-start | bytes 1048576 | tf_op jit(solution)/shard_map/all_to_all | solution.py:164
Sparse Core Ops, SparseCore 0:
  65.6 50.4 all-gather.3
Sparse Core Ops, SparseCore 1:
  117.7 28.5 reduce-scatter.1
where the time goes:
time: 216 us; the launch traced here: 215 us
  matrix products  53.2 us (25%)
  local copies, waits for them, and re-layouts  43.1 us (20%)
  waiting for transfers between devices  30.7 us (14%)
  other arithmetic  28.4 us (13%)
  starting transfers between devices  22.3 us (10%)
  blocking collectives  20.9 us (10%)
  between operations  15.9 us (7%)
    all_to_all x1, waiting for transfers between devices, mixer_half(): lax.all_to_all(heads_out.reshape(seq_rows, local_heads * HEAD_DIM), 'tp',...  25.5 us
    all_gather x1, blocking collectives, prefix(): lax.all_gather(a.astype(kind), axis)  20.9 us
    unnamed x27, local copies, waits for them, and re-layouts  13.4 us
    dot_general x1, matrix products, mixer_half(): jnp.einsum('nihd,nhde->nihe', query_decayed, block_states, precision=lax....  11.4 us
    all_to_all x1, starting transfers between devices, expert_half(): lax.all_to_all(summed_rows, 'ep', split_axis=0, concat_axis=0, tiled=True)  11 us
    dot_general x1, matrix products, mixer_half(): jnp.dot(by_rows, w_out, preferred_element_type=jnp.float32)  9.11 us
    dot_general x1, matrix products, expert_half(): up_part = jnp.dot(arrived, up_weight, preferred_element_type=jnp.float32)  8.03 us
    dot_general x1, matrix products, expert_half(): jnp.dot(arrived, gate_weight, preferred_element_type=jnp.float32)  7.83 us
  transfers between devices with their start and end apart: 5, of which 2 were waited for; matrix products, arithmetic and copies ran while one was open for 53% of the time, Pallas kernels for 0%

commit v1 on v0

--- a/solution.py
+++ b/solution.py
@@ -101,12 +101,18 @@
     heads_out = (
         gate_act * retained * inverse_rms * ret_gain.reshape(local_heads, HEAD_DIM)
     ).astype(jnp.bfloat16)
-    by_rows = lax.all_to_all(
-        heads_out.reshape(seq_rows, local_heads * HEAD_DIM),
-        "tp",
-        split_axis=0,
-        concat_axis=1,
-        tiled=True,
+    by_rows = jnp.concatenate(
+        lax.all_to_all(
+            jnp.stack(
+                jnp.split(
+                    heads_out.reshape(seq_rows, local_heads * HEAD_DIM), lax.axis_size("tp"), axis=0
+                )
+            ),
+            "tp",
+            0,
+            0,
+        ),
+        axis=1,
     )
     return jnp.dot(by_rows, w_out, preferred_element_type=jnp.float32).astype(jnp.bfloat16)
 

time: 216 us -> 209 us (0.968)
  local copies, waits for them, and re-layouts: 43.1 us -> 35.4 us
  other arithmetic: 28.4 us -> 32.2 us
    reshape x2 -> x3, local copies, waits for them, and re-layouts: 0.03 us -> 5.44 us  [the longest x1 5.42 us: mixer_half(): (within_block + carried_part).reshape(seq_rows, local_heads, HEAD_DIM)]
    add x1, local copies, waits for them, and re-layouts: 7.27 us -> 2.2 us  [mixer_half(): within_block + carried_part]
    unnamed x27 -> x24, local copies, waits for them, and re-layouts: 13.4 us -> 9.78 us
    mul x1, local copies, waits for them, and re-layouts: 2.46 us -> 0.01 us  [mixer_half(): gate_act * retained * inverse_rms * ret_gain.reshape(local_heads, HEAD_DIM)]
    all_to_all x1 -> x0, local copies, waits for them, and re-layouts: 2.36 us -> none  [mixer_half(): lax.all_to_all(heads_out.reshape(seq_rows, local_heads * HEAD_DIM), 'tp',...]
    convert_element_type x1, other arithmetic: 1.65 us -> 3.84 us  [mixer_half(): heads_out = (gate_act * retained * inverse_rms * ret_gain.reshape(local_h...]
    another operation x3 -> x4, other arithmetic: 3.22 us -> 4.8 us
  transfers between devices with their start and end apart: 5 -> 5, of which waited for: 2 -> 2; matrix products, arithmetic and copies ran while one was open for 53% -> 52% of each run, Pallas kernels for 0% -> 0%
where the time goes in v1:
time: 209 us; the launch traced here: 208 us
  matrix products  51.1 us (24%)
  local copies, waits for them, and re-layouts  35.4 us (17%)
  other arithmetic  32.2 us (15%)
  waiting for transfers between devices  30.7 us (15%)
  starting transfers between devices  21.4 us (10%)
  blocking collectives  20.9 us (10%)
  between operations  15.9 us (8%)
    all_to_all x1, waiting for transfers between devices, mixer_half(): lax.all_to_all(jnp.stack(jnp.split(heads_out.reshape(seq_rows, local_head...  25.5 us
    all_gather x1, blocking collectives, prefix(): lax.all_gather(a.astype(kind), axis)  20.9 us
    all_to_all x1, starting transfers between devices, expert_half(): lax.all_to_all(summed_rows, 'ep', split_axis=0, concat_axis=0, tiled=True)  10.1 us
    unnamed x24, local copies, waits for them, and re-layouts  9.78 us
    dot_general x1, matrix products, mixer_half(): jnp.einsum('nihd,nhde->nihe', query_decayed, block_states, precision=lax....  9.33 us
    dot_general x1, matrix products, mixer_half(): jnp.dot(by_rows, w_out, preferred_element_type=jnp.float32)  9.11 us
    dot_general x1, matrix products, expert_half(): up_part = jnp.dot(arrived, up_weight, preferred_element_type=jnp.float32)  8.06 us
    dot_general x1, matrix products, expert_half(): jnp.dot(arrived, gate_weight, preferred_element_type=jnp.float32)  7.84 us
  transfers between devices with their start and end apart: 5, of which 2 were waited for; matrix products, arithmetic and copies ran while one was open for 52% of the time, Pallas kernels for 0%

profile of v1, /device:TPU:0, one launch (start us, length us, event | category | flops | bytes accessed | tf_op | source)
XLA Modules:
  0.0 208.0 jit_solution(11516267147990734243)
XLA Ops:
  8.0 0.8 copy.171
  8.8 0.7 broadcast_multiply_fusion
  9.4 0.1 eq.15
  9.6 0.1 reduce_window_sum.48
  9.7 0.2 select_reduce_fusion
  10.0 0.1 mul.272
  10.1 0.8 scatter_custom_fusion
  10.9 1.0 fusion.51
  12.0 1.0 fusion.53
  13.0 0.9 gather_fusion
  14.0 1.6 broadcast_in_dim.38
  15.6 7.5 %all-to-all-start.1 = ((bf16[32,16,2048]{2,1,0:T(8,128)(2,1)}), bf16[32,16,2048]{2,1,0:T(8,128)(2,1)}, u32[]{:S(2)}, u32[]{:S(2)}) async-start(bf16[32,16,2048]{2,1,0:T(8,128)(2,1)} %bitcast.29), calls=%async_computation.1 | async-start | bytes 4194304 | tf_op jit(solution)/shard_map/all_to_all | solution.py:145
  23.2 2.4 %reduce-window.6 = f32[4,2,4,128]{3,2,1,0:T(4,128)S(1)} reduce-window(f32[4,2,4,128]{3,2,1,0:T(4,128)S(1)} %copy.180, f32[]{:T(128)} %constant.91.clone.1), window={size=1x1x1x128 pad=0_0x0_0x0_0x127_0}, to_apply=%region_0.0 | reduce-window | flops 520192 | bytes 32772 | tf_op jit(solution)/shard_map/reduce-window
  25.6 0.2 slice_reduce_fusion
  25.8 0.7 reduce-window.9
  26.6 0.2 slice_reduce_fusion.1
  26.9 2.9 %copy.143 = bf16[2048,512]{0,1:T(8,128)(2,1)S(1)} copy(bf16[2048,512]{1,0:T(8,128)(2,1)} %param.18) | data formatting | bytes 4194304 | tf_op args[0]
  29.8 2.5 %convert.17 = f32[2048,2,256]{0,2,1:T(8,128)} convert(bf16[2048,2,256]{0,2,1:T(8,128)(2,1)S(1)} %bitcast.103) | non-fusion elementwise | flops 1048576 | bytes 6291456 | tf_op jit(solution)/shard_map/reshape | solution.py:58
  32.3 2.9 %copy.148 = bf16[2048,512]{0,1:T(8,128)(2,1)S(1)} copy(bf16[2048,512]{1,0:T(8,128)(2,1)} %param.19) | data formatting | bytes 4194304 | tf_op args[1]
  35.2 0.5 convert.18
  35.7 3.7 %multiply_cosine_fusion = (f32[2048,128]{0,1:T(8,128)S(1)}, f32[2048,128]{0,1:T(8,128)S(1)}) fusion(f32[128]{0:T(128)S(1)} %multiply_power_fusion, f32[2048]{0:T(1024)S(1)} %add_convert_fusion.1), kind=kLoop, calls=%fused_computation.62 | loop fusion | flops 262144 | bytes 2105856 | tf_op jit(solution)/shard_map/cos | solution.py:36
  39.5 3.1 %multiply_subtract_fusion = (f32[2048,2,128]{0,2,1:T(8,128)}, f32[2048,2,128]{0,2,1:T(8,128)S(1)}, bf16[2048,2,128]{0,2,1:T(8,128)(2,1)S(1)}, bf16[2048,2,128]{0,2,1:T(8,128)(2,1)}) fusion(f32[2048,2,256]{0,2,1:T(8,128)S(1)} %convert.18, f32[2048,128]{0,1:T(8,128)S(1)} %get-tuple-element.188, f32[2048,128]{0,1:T(8,128)S(1)} %get-tuple-element.187, ...), kind=kLoop, calls=%fused_computation.54 | loop fusion | flops 7340032 | bytes 16777216 | tf_op jit(solution)/shard_map/sub | solution.py:40
  42.5 2.9 %copy.149 = f32[2048,2,128]{2,0,1:T(8,128)} copy(f32[2048,2,128]{0,2,1:T(8,128)} %get-tuple-element.175) | data formatting | bytes 4194304 | tf_op jit(solution)/shard_map/sub | solution.py:40
  45.4 1.8 copy.150
  47.3 4.2 %reshape.258 = bf16[4,512,2,256]{3,2,1,0:T(2,128)(2,1)} reshape(bf16[2048,512]{1,0:T(8,128)(2,1)} %param.20) | data formatting | bytes 4194304 | tf_op jit(solution)/shard_map/reshape | solution.py:66
  51.4 5.1 %fusion.36 = f32[4,2,256,256]{3,2,1,0:T(8,128)} fusion(f32[4,512,2]{1,2,0:T(2,128)S(1)} %copy.158, bf16[4,512,2,256]{3,2,1,0:T(2,128)(2,1)} %reshape.258, f32[4,512,2,128]{3,1,0,2:T(8,128)} %bitcast.113, f32[4,512,2,128]{3,1,0,2:T(8,128)S(1)} %bitcast.112), kind=kOutput, calls=%fused_computation.46 | convolution fusion | flops 543162368 | bytes 8404992 | tf_op jit(solution)/shard_map/njhd,njhe->nhde/dot_general | solution.py:83
  56.6 8.1 %while.26 = (s32[]{:T(128)}, f32[2,256,256]{2,1,0:T(8,128)S(1)}, f32[4,2,256,256]{3,2,1,0:T(8,128)}, f32[4,2]{1,0:T(4,128)S(1)}, f32[4,2,256,256]{3,2,1,0:T(8,128)}, /*index=5*/s32[]{:T(128)}, s32[]{:T(128)}) while((s32[]{:T(128)}, f32[2,256,256]{2,1,0:T(8,128)S(1)}, f32[4,2,256,256]{3,2,1,0:T(8,128)}, f32[4,2]{1,0:T(4,128)S(1)}, ...), condition=%wide.region_3.4_spmd.clone, body=%wide.region_2.3_spmd.clone.sunk | while | flops 524291 | bytes 2622072 | solution.py:87
  56.6 0.8 bitcast_dynamic-update-slice_fusion.2
  57.5 1.2 bitcast_add_fusion.4
  58.6 0.8 bitcast_dynamic-update-slice_fusion.2
  59.5 1.2 bitcast_add_fusion.4
  60.7 0.8 bitcast_dynamic-update-slice_fusion.2
  61.5 1.2 bitcast_add_fusion.4
  62.7 0.8 bitcast_dynamic-update-slice_fusion.2
  63.5 1.2 bitcast_add_fusion.4
  64.7 0.7 convert_element_type.96
  65.5 0.2 reduce_window_sum.47
  65.7 0.2 fusion.55
  65.9 20.9 %all-gather.1 = bf16[8,1,2]{2,1,0:T(2,128)(2,1)S(1)} all-gather(bf16[1,1,2]{2,1,0:T(2,128)(2,1)S(1)} %bitcast.127), channel_id=1, replica_groups=mesh['ep'=8,'tp'=4] {'ep'}, dimensions={0}, use_global_device_ids=true | all-gather | bytes 36 | tf_op jit(solution)/shard_map/all_gather | solution.py:14
  86.8 0.1 copy.163
  86.9 0.7 copy.144
  87.6 1.4 copy.145
  88.9 0.1 copy.162
  89.1 2.9 %copy.142 = bf16[2048,512]{0,1:T(8,128)(2,1)S(1)} copy(bf16[2048,512]{1,0:T(8,128)(2,1)} %param.21) | data formatting | bytes 4194304 | tf_op args[3]
  92.1 7.5 %fusion.14 = f32[4,2,512,256]{3,2,1,0:T(8,128)} fusion(f32[4,2,512]{2,1,0:T(2,128)S(1)} %reshape.302, pred[512,512]{1,0:T(8,128)(4,1)S(1)} %iota_compare_fusion, bf16[4,512,2,256]{3,2,1,0:T(2,128)(2,1)} %reshape.258, f32[4,512,2,128]{3,1,0,2:T(8,128)} %bitcast.114, f32[4,512,2,128]{3,1,0,2:T(8,128)} %bitcast.111, bf16[4,512,2,128]{3,1,0,2:T(8,128)(2,1)} %bitcast.108, ...), kind=kOutput, calls=%fused_computation.26 | convolution fusion | flops 2165309440 | bytes 12861440 | tf_op jit(solution)/shard_map/nhij,njhe->nihe/dot_general | solution.py:76
  99.7 7.8 %fusion.6 = f32[512,1792]{1,0:T(8,128)S(1)} fusion(bf16[512,2048]{1,0:T(8,128)(2,1)} %bitcast.30, bf16[1,2048,1792]{2,1,0:T(8,128)(2,1)} %param.29), kind=kOutput, calls=%fused_computation.16 | convolution fusion | flops 3758096384 | bytes 13107200 | tf_op jit(solution)/shard_map/dot_general | solution.py:152
  107.5 8.1 %multiply_convert_fusion.3 = bf16[512,1792]{1,0:T(8,128)(2,1)S(1)} fusion(f32[512,1792]{1,0:T(8,128)S(1)} %fusion.6, bf16[512,2048]{1,0:T(8,128)(2,1)} %bitcast.30, bf16[1,2048,1792]{2,1,0:T(8,128)(2,1)} %param.30), kind=kOutput, calls=%fused_computation.41 | convolution fusion | flops 3763601408 | bytes 14942208 | tf_op jit(solution)/shard_map/dot_general | solution.py:153
  115.6 4.2 %fusion.31 = bf16[4,8,16,2048]{3,2,0,1:T(8,128)(2,1)S(1)} fusion(bf16[8,4,16,1792]{3,2,1,0:T(8,128)(2,1)S(1)} %bitcast.130, bf16[1,1792,2048]{2,1,0:T(8,128)(2,1)S(1)} %bitcast.129), kind=kOutput, calls=%fused_computation.45 | convolution fusion | flops 3759144960 | bytes 11272192 | tf_op jit(solution)/shard_map/elcf,fd->lecd/dot_general | solution.py:159
  119.8 1.5 copy.172
  121.5 0.2 while.25
  121.7 9.3 %multiply_reduce_fusion = (f32[4,512,2]{1,2,0:T(2,128)S(1)}, f32[4,512,2,256]{3,1,2,0:T(8,128)S(1)}) fusion(f32[4,512,2]{1,2,0:T(2,128)S(1)} %copy.165, f32[4,2,256,256]{3,2,1,0:T(8,128)} %get-tuple-element.74, f32[2,256,256]{2,1,0:T(8,128)S(1)} %get-tuple-element.76, f32[4,2]{1,0:T(4,128)S(1)} %copy.162, f32[4,2,512,256]{3,2,1,0:T(8,128)} %fusion.14, ...), kind=kOutput, calls=%fused_computation.31 | convolution fusion | flops 3231707136 | bytes 13140000 | tf_op jit(solution)/shard_map/nihd,nhde->nihe/dot_general | solution.py:95
  131.0 2.2 %copy.168 = f32[4,512,2,256]{3,1,0,2:T(8,128)} copy(f32[4,512,2,256]{3,1,2,0:T(8,128)S(1)} %get-tuple-element.190) | data formatting | bytes 8388608 | tf_op jit(solution)/shard_map/add | solution.py:98
  133.2 5.4 %copy.169 = f32[2048,2,256]{0,2,1:T(8,128)} copy(f32[2048,2,256]{2,0,1:T(8,128)} %bitcast.100) | data formatting | bytes 8388608 | tf_op jit(solution)/shard_map/reshape | solution.py:98
  138.7 3.8 %fusion.22 = bf16[2048,2,256]{0,2,1:T(8,128)(2,1)S(1)} fusion(f32[2048,2,256]{0,2,1:T(8,128)} %copy.169, bf16[2048,2,256]{0,2,1:T(8,128)(2,1)S(1)} %bitcast.102, f32[2,256]{1,0:T(2,128)S(1)} %mul.262, f32[2048,2]{0,1:T(2,128)S(1)} %bitcast.122), kind=kLoop, calls=%fused_computation.39 | loop fusion | flops 9437184 | bytes 8407040 | tf_op jit(solution)/shard_map/convert_element_type | solution.py:103
  142.5 0.2 fusion.64
  142.7 1.6 pad_maximum_fusion.2
  144.3 3.7 %all-to-all-start = ((bf16[4,512,512]{1,2,0:T(8,128)(2,1)}), bf16[4,512,512]{1,2,0:T(8,128)(2,1)S(1)}, u32[]{:S(2)}, u32[]{:S(2)}) async-start(bf16[4,512,512]{1,2,0:T(8,128)(2,1)} %pad_maximum_fusion.2), calls=%async_computation | async-start | bytes 4194304 | tf_op jit(solution)/shard_map/all_to_all | solution.py:105
  148.1 25.5 %all-to-all-done = bf16[4,512,512]{1,2,0:T(8,128)(2,1)S(1)} async-done(((bf16[4,512,512]{1,2,0:T(8,128)(2,1)}), bf16[4,512,512]{1,2,0:T(8,128)(2,1)S(1)}, u32[]{:S(2)}, u32[]{:S(2)}) %all-to-all-start) | async-done | bytes 2097184 | tf_op jit(solution)/shard_map/all_to_all | solution.py:105
  173.7 10.1 %all-to-all-start.2 = ((bf16[8,16,2048]{2,1,0:T(8,128)(2,1)}), bf16[8,16,2048]{2,1,0:T(8,128)(2,1)S(1)}, u32[]{:S(2)}, u32[]{:S(2)}) async-start(bf16[8,16,2048]{2,1,0:T(8,128)(2,1)} %bitcast.121), calls=%async_computation.3 | async-start | bytes 1048576 | tf_op jit(solution)/shard_map/all_to_all | solution.py:170
  183.8 9.1 %convolution_convert_fusion = bf16[512,2048]{1,0:T(8,128)(2,1)} fusion(bf16[512,2048]{0,1:T(8,128)(2,1)S(1)} %bitcast.115, bf16[2048,2048]{1,0:T(8,128)(2,1)} %param.24), kind=kOutput, calls=%fused_computation.43 | convolution fusion | flops 4296015872 | bytes 12582912 | tf_op jit(solution)/shard_map/dot_general | solution.py:117
  192.9 5.1 %all-to-all-done.2 = bf16[8,16,2048]{2,1,0:T(8,128)(2,1)S(1)} async-done(((bf16[8,16,2048]{2,1,0:T(8,128)(2,1)}), bf16[8,16,2048]{2,1,0:T(8,128)(2,1)S(1)}, u32[]{:S(2)}, u32[]{:S(2)}) %all-to-all-start.2) | async-done | bytes 524320 | tf_op jit(solution)/shard_map/all_to_all | solution.py:170
  198.0 0.7 gather_fusion.1
  198.8 0.3 reshape.271
  199.1 1.4 multiply_reduce_fusion.1
  (59 shorter events, 1.0 us)
Async XLA Ops:
  15.6 7.5 %copy-start.4 = (f32[2048,2]{0,1:T(2,128)S(1)}, f32[2048,2]{0,1:T(2,128)}, u32[]{:S(2)}) copy-start(f32[2048,2]{0,1:T(2,128)} %param.22) | copy-start | bytes 49156
  15.6 84.1 %all-to-all-start.1 = ((bf16[32,16,2048]{2,1,0:T(8,128)(2,1)}), bf16[32,16,2048]{2,1,0:T(8,128)(2,1)}, u32[]{:S(2)}, u32[]{:S(2)}) async-start(bf16[32,16,2048]{2,1,0:T(8,128)(2,1)} %bitcast.29), calls=%async_computation.1 | async-start | bytes 4194304 | tf_op jit(solution)/shard_map/all_to_all | solution.py:145
  23.0 98.4 %all-gather.4.cloned.1.call-start = ((), (), s32[]{:S(2)}) async-start(), calls=%async_computation.5 | async-start | bytes 2359296 | tf_op jit(solution)/shard_map/all_gather | solution.py:14
  35.2 4.2 %copy-start = (f32[2048,2,256]{0,2,1:T(8,128)S(1)}, f32[2048,2,256]{0,2,1:T(8,128)}, u32[]{:S(2)}) copy-start(f32[2048,2,256]{0,2,1:T(8,128)} %convert.17) | copy-start | bytes 12582916
  47.3 4.2 %copy-start.3 = (f32[2048,2,128]{2,0,1:T(8,128)S(1)}, f32[2048,2,128]{2,0,1:T(8,128)}, u32[]{:S(2)}) copy-start(f32[2048,2,128]{2,0,1:T(8,128)} %copy.149) | copy-start | bytes 6291460
  56.6 30.3 %copy-start.1 = (bf16[2048,2,128]{0,2,1:T(8,128)(2,1)S(1)}, bf16[2048,2,128]{0,2,1:T(8,128)(2,1)}, u32[]{:S(2)}) copy-start(bf16[2048,2,128]{0,2,1:T(8,128)(2,1)} %get-tuple-element.184) | copy-start | bytes 3145732
  65.5 108.2 %reduce-scatter.2.cloned.1.call-start = ((), (), s32[]{:S(2)}) async-start(), calls=%async_computation.4 | async-start | bytes 2621440 | tf_op jit(solution)/shard_map/reduce_scatter | solution.py:162
  87.6 4.6 %copy-start.2 = (bf16[2048,2,128]{2,0,1:T(8,128)(2,1)}, bf16[2048,2,128]{2,0,1:T(8,128)(2,1)S(1)}, u32[]{:S(2)}) copy-start(bf16[2048,2,128]{2,0,1:T(8,128)(2,1)S(1)} %copy.144) | copy-start | bytes 3145732
  89.1 3.0 %copy-start.5 = (f32[512]{0:T(512)S(1)}, f32[512]{0:T(512)}, u32[]{:S(2)}) copy-start(f32[512]{0:T(512)} %param.23) | copy-start | bytes 6148
  99.7 15.9 %slice-start = ((s8[7340032]{0:T(1024)(128)(4,1)}), s8[4194304]{0:T(1024)(128)(4,1)S(1)}, s32[]{:S(2)}) async-start(s8[7340032]{0:T(1024)(128)(4,1)} %bitcast.128), calls=%async_computation.6 | async-start | bytes 8388608
  107.5 8.1 %slice-start.1 = ((s8[7340032]{0:T(1024)(128)(4,1)}), s8[3145728]{0:T(1024)(128)(4,1)S(1)}, s32[]{:S(2)}) async-start(s8[7340032]{0:T(1024)(128)(4,1)} %bitcast.128), calls=%async_computation.7 | async-start | bytes 6291456
  144.3 3.8 %copy-start.6 = (f32[32,2]{0,1:T(2,128)S(1)}, f32[32,2]{0,1:T(2,128)}, u32[]{:S(2)}) copy-start(f32[32,2]{0,1:T(2,128)} %param.27) | copy-start | bytes 772
  144.3 29.4 %all-to-all-start = ((bf16[4,512,512]{1,2,0:T(8,128)(2,1)}), bf16[4,512,512]{1,2,0:T(8,128)(2,1)S(1)}, u32[]{:S(2)}, u32[]{:S(2)}) async-start(bf16[4,512,512]{1,2,0:T(8,128)(2,1)} %pad_maximum_fusion.2), calls=%async_computation | async-start | bytes 4194304 | tf_op jit(solution)/shard_map/all_to_all | solution.py:105
  173.7 24.4 %all-to-all-start.2 = ((bf16[8,16,2048]{2,1,0:T(8,128)(2,1)}), bf16[8,16,2048]{2,1,0:T(8,128)(2,1)S(1)}, u32[]{:S(2)}, u32[]{:S(2)}) async-start(bf16[8,16,2048]{2,1,0:T(8,128)(2,1)} %bitcast.121), calls=%async_computation.3 | async-start | bytes 1048576 | tf_op jit(solution)/shard_map/all_to_all | solution.py:170
Sparse Core Ops, SparseCore 0:
  65.6 50.4 all-gather.3
Sparse Core Ops, SparseCore 1:
  121.5 28.3 reduce-scatter.1
